TPU v7x, 512 devices: a whole 4x4x16 slice. The times are simulated.
512 devices in a mesh: ep: 32 (over z, core), tp: 16 (over y, x).
Axes of the slice: x: 4, y: 4, z: 16, core: 2. Of those that a mesh axis runs over, the one named last changes fastest.
Arguments:
- tokens: bfloat16 [512, 2048], P('ep'), may hold values from -6 to 6
- attn_gain: float32 [2048], replicated, may hold values from 0.1 to 1.9
- query_weight: bfloat16 [2048, 2048], P('ep', 'tp'), may hold values from -0.125 to 0.125
- key_weight: bfloat16 [2048, 2048], P('ep', 'tp'), may hold values from -0.125 to 0.125
- value_weight: bfloat16 [2048, 2048], P('ep', 'tp'), may hold values from -0.125 to 0.125
- forget_weight: bfloat16 [2048, 16], P(None, 'tp'), may hold values from -0.125 to 0.125
- forget_bias: float32 [16], P('tp'), may hold values from -1 to 2
- cache_keys: bfloat16 [512, 16, 384, 128], P('ep', 'tp'), may hold values from -240 to 240
- cache_values: bfloat16 [512, 16, 384, 128], P('ep', 'tp'), may hold values from -6 to 6
- cache_gates: float32 [512, 16, 384], P('ep', 'tp'), may hold values from -768 to 0, as said below
- lengths: int32 [512], P('ep'), may hold values from 1 to 384
- output_weight: bfloat16 [2048, 2048], P('tp', 'ep'), may hold values from -0.125 to 0.125
- ffn_gain: float32 [2048], replicated, may hold values from 0.1 to 1.9
- dense_gate_proj: bfloat16 [2048, 2048], P('ep', 'tp'), may hold values from -0.125 to 0.125
- dense_up_proj: bfloat16 [2048, 2048], P('ep', 'tp'), may hold values from -0.125 to 0.125
- dense_down_proj: bfloat16 [2048, 2048], P('tp', 'ep'), may hold values from -0.125 to 0.125
- dense_mix: bfloat16 [2048], replicated, may hold values from -0.125 to 0.125
- expert_ids: int32 [512, 2], P('ep'), may hold values from 0 to 31, as said below
- group_prob: float32 [512], P('ep'), may hold values from 0.25 to 1
- pair_prob: float32 [512, 2], P('ep'), may hold values from 0.05 to 1
- expert_gate: bfloat16 [32, 2048, 2048], P('ep', None, 'tp'), may hold values from -0.125 to 0.125
- expert_up: bfloat16 [32, 2048, 2048], P('ep', None, 'tp'), may hold values from -0.125 to 0.125
- expert_down: bfloat16 [32, 2048, 2048], P('ep', 'tp'), may hold values from -0.125 to 0.125
Outputs:
- mixed_out: bfloat16 [512, 2048], P('ep')
Inputs may be any that keep to these rules, and one draw needn't show every extreme that they name: `expert_ids`: each row names two different experts of one group, the groups being 4 runs of consecutive ids. In each aligned block of 16 rows (the rows of one index of ep) no expert is named more than 2 times, and some expert exactly 2 times. `cache_gates`: along positions the values never rise.
All inputs are finite; a program needn't handle non-finite values.
Results may differ from a plain program's by a relative error of at most 0.014.
Values may be sent and summed in bfloat16 or wider, within the bound.
No kernel may reach another device: no remote copies, remote signals or barrier semaphores. Data moves between devices by JAX's collectives and lax.ppermute only.
A program may use at most 64 MiB of HBM per device.

v0:
```python
import math
import jax
import jax.numpy as jnp
from jax import lax
from jax.sharding import Mesh
from jax.sharding import PartitionSpec as P

EP = ("ep_0", "ep_1")
EPSILON = 1e-06


def sent_together(arrays, axis, dim, along):
    widths = [a.shape[along] for a in arrays]
    both = jnp.concatenate(arrays, axis=along)
    filled = lax.all_gather(both, axis, axis=dim, tiled=True)
    return tuple(jnp.split(filled, [sum(widths[:k]) for k in range(1, len(widths))], axis=along))


def from_everyone(array, axis):
    copies = jnp.broadcast_to(array, (lax.axis_size(axis), *array.shape))
    return lax.all_to_all(copies, axis, split_axis=0, concat_axis=0, tiled=True)


def laid_out(pieces, dim):
    lengths = list(pieces.shape[1:])
    lengths[dim] *= pieces.shape[0]
    return jnp.moveaxis(pieces, 0, dim).reshape(lengths)


def collect(array, axis, dim):
    pieces = from_everyone(array, axis)
    return laid_out(pieces, dim)


def taken_together(array, axis):
    everything = from_everyone(array, axis)
    return jnp.sum(everything.astype(jnp.float32), axis=0)


def gather_in_order(array, axes, sequence):
    pieces = array[None]
    for k in sequence:
        pieces = lax.all_gather(pieces, axes[k], axis=0, tiled=True)
    held = [lax.axis_size(axes[k]) for k in reversed(sequence)]
    pieces = pieces.reshape(*held, *array.shape)
    turned = sorted(range(len(sequence)), key=lambda place: sequence[len(sequence) - 1 - place])
    return pieces.transpose(*turned, *range(len(sequence), pieces.ndim)).reshape(-1, *array.shape)


def gathered_by_axis(array, axes, sequence, dim):
    return laid_out(gather_in_order(array, axes, sequence), dim)


def rms_scale(values, norm_gain):
    widened = values.astype(jnp.float32)
    return (
        widened
        * lax.rsqrt(jnp.mean(widened * widened, axis=-1, keepdims=True) + EPSILON)
        * norm_gain
    )


def attend(queries, keys_new, values_new, key_cache, value_cache, gate_cache, lengths, log_forget):
    cache_span = key_cache.shape[2]
    score_scale = 1.0 / math.sqrt(key_cache.shape[3])
    positions = jnp.arange(cache_span, dtype=jnp.int32)
    live_mask = positions[None, :] < lengths[:, None]
    last_mask = positions[None, :] == lengths[:, None] - 1
    last_gate = jnp.sum(jnp.where(last_mask[:, None, :], gate_cache, 0.0), axis=-1)
    gate_now = last_gate + log_forget
    scores = (
        jnp.einsum("shd,shpd->shp", queries, key_cache, preferred_element_type=jnp.float32)
        * score_scale
    )
    scores = scores + gate_now[:, :, None] - gate_cache
    scores = jnp.where(live_mask[:, None, :], scores, -jnp.inf)
    own_score = (
        jnp.sum(queries.astype(jnp.float32) * keys_new.astype(jnp.float32), axis=-1) * score_scale
    )
    row_top = jnp.maximum(jnp.max(scores, axis=-1), own_score)
    raised = jnp.exp(scores - row_top[:, :, None])
    own_raised = jnp.exp(own_score - row_top)
    totals = jnp.sum(raised, axis=-1) + own_raised
    weights_low = (raised / totals[:, :, None]).astype(jnp.bfloat16)
    own_prob = (own_raised / totals).astype(jnp.bfloat16)
    attended = jnp.einsum(
        "shp,shpd->shd", weights_low, value_cache, preferred_element_type=jnp.float32
    )
    attended = attended + own_prob.astype(jnp.float32)[:, :, None] * values_new.astype(jnp.float32)
    return attended.astype(jnp.bfloat16)


def column_fold(source, pieces):
    return tuple(
        (
            jnp.dot(source, weight_piece, preferred_element_type=jnp.float32)
            for weight_piece in pieces
        )
    )


def right_product(left_rows, weight_piece):
    return jnp.dot(left_rows, weight_piece, preferred_element_type=jnp.float32)


def shards(
    tokens,
    attn_gain,
    query_weight,
    key_weight,
    value_weight,
    forget_weight,
    forget_bias,
    cache_keys,
    cache_values,
    cache_gates,
    lengths,
    output_weight,
    ffn_gain,
    dense_gate_proj,
    dense_up_proj,
    dense_down_proj,
    dense_mix,
    expert_ids,
    group_prob,
    pair_prob,
    expert_gate,
    expert_up,
    expert_down,
):
    seq_count = tokens.shape[0]
    head_count = cache_keys.shape[1]
    head_size = cache_keys.shape[3]
    normed = rms_scale(tokens, attn_gain).astype(jnp.bfloat16)
    projected = column_fold(
        normed, sent_together((query_weight, key_weight, value_weight), EP, 0, 1)
    )
    queries = projected[0].astype(jnp.bfloat16).reshape(seq_count, head_count, head_size)
    keys_new = projected[1].astype(jnp.bfloat16).reshape(seq_count, head_count, head_size)
    values_new = projected[2].astype(jnp.bfloat16).reshape(seq_count, head_count, head_size)
    log_forget = jax.nn.log_sigmoid(
        jnp.dot(normed, forget_weight, preferred_element_type=jnp.float32) + forget_bias
    )
    attended = attend(
        queries, keys_new, values_new, cache_keys, cache_values, cache_gates, lengths, log_forget
    )
    attended = attended.reshape(seq_count, head_count * head_size)
    head_terms = right_product(attended, collect(output_weight, EP, 1))
    mixed_heads = taken_together(head_terms.astype(jnp.bfloat16), "tp").astype(jnp.float32)
    residual = (tokens.astype(jnp.float32) + mixed_heads).astype(jnp.bfloat16)
    ffn_in = rms_scale(residual, ffn_gain).astype(jnp.bfloat16)
    dense_parts = column_fold(ffn_in, sent_together((dense_gate_proj, dense_up_proj), EP, 0, 1))
    dense_hidden = (jax.nn.silu(dense_parts[0]) * dense_parts[1]).astype(jnp.bfloat16)
    dense_terms = right_product(dense_hidden, gathered_by_axis(dense_down_proj, EP, (0, 1), 1))
    mix = jax.nn.sigmoid(jnp.dot(ffn_in, dense_mix, preferred_element_type=jnp.float32))
    expert_count = lax.axis_size(EP) * expert_gate.shape[0]
    capacity = 4 * seq_count // expert_count
    slot_total = expert_count * capacity
    picks = expert_ids.reshape(-1)
    expert_grid = jnp.arange(expert_count, dtype=jnp.int32)
    pick_onehot = (picks[:, None] == expert_grid[None, :]).astype(jnp.int32)
    earlier = jnp.cumsum(pick_onehot, axis=0) - pick_onehot
    slot_rank = jnp.sum(earlier * pick_onehot, axis=1)
    destination = (picks * capacity + slot_rank).reshape(seq_count, 2)
    slot_grid = jnp.arange(slot_total, dtype=jnp.int32)
    select_first = (destination[:, 0:1] == slot_grid[None, :]).astype(jnp.bfloat16)
    select_second = (destination[:, 1:2] == slot_grid[None, :]).astype(jnp.bfloat16)
    selector = select_first + select_second
    outbound = jnp.einsum("sk,sd->kd", selector, ffn_in, preferred_element_type=jnp.float32)
    outbound = outbound.astype(jnp.bfloat16).reshape(expert_count, capacity, ffn_in.shape[1])
    arrived = lax.all_to_all(outbound, EP, split_axis=0, concat_axis=0, tiled=True)
    sources, slots_now, feature = arrived.shape
    row_data = arrived.reshape(sources * slots_now, feature)
    gate_part = jnp.dot(row_data, expert_gate[0], preferred_element_type=jnp.float32)
    up_part = jnp.dot(row_data, expert_up[0], preferred_element_type=jnp.float32)
    expert_hidden = (jax.nn.silu(gate_part) * up_part).astype(jnp.bfloat16)
    partial_out = jnp.dot(expert_hidden, expert_down[0], preferred_element_type=jnp.float32)
    returned = lax.all_to_all(
        partial_out.reshape(sources, slots_now, feature).astype(jnp.bfloat16),
        EP,
        split_axis=0,
        concat_axis=0,
        tiled=True,
    ).astype(jnp.float32)
    returned = returned.reshape(slot_total, ffn_in.shape[1])
    routes = group_prob[:, None] * pair_prob / jnp.sum(pair_prob, axis=1, keepdims=True)
    first_back = returned[destination[:, 0]]
    second_back = returned[destination[:, 1]]
    side_total = (
        routes[:, 0:1] * first_back + routes[:, 1:2] * second_back + mix[:, None] * dense_terms
    )
    side_total = taken_together(side_total.astype(jnp.bfloat16), "tp").astype(jnp.float32)
    result = residual.astype(jnp.float32) + side_total
    return result.astype(jnp.bfloat16)


def solution(mesh):
    finer = Mesh(mesh.devices.reshape(16, 2, mesh.shape["tp"]), ("ep_0", "ep_1", "tp"))
    in_specs = (
        P(EP, None),
        P(),
        P(EP, "tp"),
        P(EP, "tp"),
        P(EP, "tp"),
        P(None, "tp"),
        P("tp"),
        P(EP, "tp", None, None),
        P(EP, "tp", None, None),
        P(EP, "tp", None),
        P(EP),
        P("tp", EP),
        P(),
        P(EP, "tp"),
        P(EP, "tp"),
        P("tp", EP),
        P(),
        P(EP, None),
        P(EP),
        P(EP, None),
        P(EP, None, "tp"),
        P(EP, None, "tp"),
        P(EP, "tp", None),
    )
    out_specs = P(EP, None)
    return jax.shard_map(
        shards, mesh=finer, in_specs=in_specs, out_specs=out_specs, check_vma=False
    )
```

profile of v0, /device:TPU:1, one launch (start us, length us, event | category | flops | bytes accessed | tf_op | source)
XLA Modules:
  0.0 240.2 jit_solution(12965718424162420117)
XLA Ops:
  6.6 1.5 pad_maximum_fusion
  8.1 1.6 broadcast_in_dim.17
  9.7 16.7 %all-to-all-start = ((bf16[32,128,64]{1,2,0:T(8,128)(2,1)}), bf16[32,128,64]{1,2,0:T(8,128)(2,1)S(1)}, u32[]{:S(2)}, u32[]{:S(2)}) async-start(bf16[32,128,64]{1,2,0:T(8,128)(2,1)} %broadcast_in_dim.17), calls=%async_computation | async-start | bytes 1048576 | tf_op jit(solution)/shard_map/all_to_all | solution.py:21
  27.1 0.1 fusion.33
  27.3 0.3 fusion.45
  27.6 0.2 fusion.65
  27.8 63.6 %all-gather.4.cloned.1.call-done = bf16[2048,384]{1,0:T(8,128)(2,1)} async-done(((bf16[64,384]{1,0:T(8,128)(2,1)}), bf16[2048,384]{1,0:T(8,128)(2,1)}) %all-gather.4.cloned.1.call-update) | async-done | bytes 1572880 | tf_op jit(solution)/shard_map/all_gather | solution.py:15
  91.4 1.4 convolution_convert_fusion.5
  92.8 1.4 fusion.14
  94.2 0.6 fusion.4
  94.9 0.3 fusion.82
  95.2 0.3 fusion.70
  95.6 0.4 fusion.2
  96.0 1.5 convolution_convert_fusion.2
  97.5 1.1 broadcast_in_dim.18
  98.6 6.6 %all-to-all-start.1 = ((bf16[16,16,2048]{2,1,0:T(8,128)(2,1)}), bf16[16,16,2048]{2,1,0:T(8,128)(2,1)S(1)}, u32[]{:S(2)}, u32[]{:S(2)}) async-start(bf16[16,16,2048]{2,1,0:T(8,128)(2,1)} %broadcast_in_dim.18), calls=%async_computation.1 | async-start | bytes 2097152 | tf_op jit(solution)/shard_map/all_to_all | solution.py:21
  105.3 0.1 copy.61
  105.4 0.1 eq.65
  105.6 0.2 select_reduce_fusion
  105.8 0.1 reduce_sum.90
  105.8 0.1 copy.62
  106.0 15.7 %all-to-all-done.1 = bf16[16,16,2048]{2,1,0:T(8,128)(2,1)S(1)} async-done(((bf16[16,16,2048]{2,1,0:T(8,128)(2,1)}), bf16[16,16,2048]{2,1,0:T(8,128)(2,1)S(1)}, u32[]{:S(2)}, u32[]{:S(2)}) %all-to-all-start.1) | async-done | bytes 1048608 | tf_op jit(solution)/shard_map/all_to_all | solution.py:21
  121.7 0.1 convert_reduce_fusion.1
  121.8 0.1 fusion.37
  122.0 0.3 convolution_convert_fusion.1
  122.3 0.9 reshape.216
  123.2 10.1 %all-to-all-start.2 = ((bf16[32,2,2048]{2,1,0:T(2,128)(2,1)}), bf16[32,2,2048]{2,1,0:T(2,128)(2,1)S(1)}, u32[]{:S(2)}, u32[]{:S(2)}) async-start(bf16[32,2,2048]{2,1,0:T(2,128)(2,1)} %reshape.216), calls=%async_computation.2 | async-start | bytes 524288 | tf_op jit(solution)/shard_map/all_to_all | solution.py:171
  133.3 0.6 pad_maximum_fusion.1
  134.0 32.8 %all-gather = bf16[2048,64]{0,1:T(8,128)(2,1)S(1)} all-gather(bf16[128,64]{0,1:T(8,128)(2,1)S(1)} %copy-done.6), channel_id=2, replica_groups=mesh['ep_0'=16,'ep_1'=2,'tp'=16] {'ep_0'}, dimensions={0}, use_global_device_ids=true | all-gather | bytes 278528 | tf_op jit(solution)/shard_map/all_gather | solution.py:43
  166.9 7.8 %all_gather.15 = bf16[32,128,64]{1,0,2:T(8,128)(2,1)S(1)} all-gather(bf16[16,128,64]{1,0,2:T(8,128)(2,1)S(1)} %bitcast.83), channel_id=1, replica_groups=mesh['ep_0'=16,'ep_1'=2,'tp'=16] {'ep_1'}, dimensions={0}, use_global_device_ids=true | all-gather | bytes 786432 | tf_op jit(solution)/shard_map/all_gather | solution.py:43
  174.7 0.2 copy.66
  174.9 0.1 reshape.217
  175.1 0.2 fusion.31
  175.3 1.3 fusion.6
  176.6 0.2 convolution_convert_fusion
  176.8 1.0 copy.64
  177.8 10.6 %all-to-all-start.3 = ((bf16[32,2,2048]{2,1,0:T(2,128)(2,1)}), bf16[32,2,2048]{2,1,0:T(2,128)(2,1)S(1)}, u32[]{:S(2)}, u32[]{:S(2)}) async-start(bf16[32,2,2048]{2,1,0:T(2,128)(2,1)} %copy.64), calls=%async_computation.3 | async-start | bytes 524288 | tf_op jit(solution)/shard_map/all_to_all | solution.py:178
  188.5 0.2 fusion.18
  188.7 17.2 %all-gather.6.cloned.1.call-done = bf16[2048,256]{1,0:T(8,128)(2,1)} async-done(((bf16[64,256]{1,0:T(8,128)(2,1)}), bf16[2048,256]{1,0:T(8,128)(2,1)}) %all-gather.6.cloned.1.call-update) | async-done | bytes 1048592 | tf_op jit(solution)/shard_map/all_gather | solution.py:15
  205.9 1.3 fusion.23
  207.2 3.8 %all-to-all-done.3 = bf16[32,2,2048]{2,1,0:T(2,128)(2,1)S(1)} async-done(((bf16[32,2,2048]{2,1,0:T(2,128)(2,1)}), bf16[32,2,2048]{2,1,0:T(2,128)(2,1)S(1)}, u32[]{:S(2)}, u32[]{:S(2)}) %all-to-all-start.3) | async-done | bytes 262176 | tf_op jit(solution)/shard_map/all_to_all | solution.py:178
  211.1 0.6 gather_fusion
  211.7 0.6 gather_fusion.1
  212.3 1.5 fusion.1
  213.8 0.1 broadcast_in_dim.20
  213.9 18.7 %all_to_all.25 = bf16[16,16,2048]{2,1,0:T(8,128)(2,1)S(1)} all-to-all(bf16[16,16,2048]{2,1,0:T(8,128)(2,1)S(1)} %broadcast_in_dim.20), channel_id=1, replica_groups=mesh['ep_0'=16,'ep_1'=2,'tp'=16] {'tp'}, dimensions={0} | all-to-all | bytes 2097152 | tf_op jit(solution)/shard_map/all_to_all | solution.py:21
  232.6 0.1 convert_reduce_fusion
  232.8 0.6 fusion.40
  (57 shorter events, 0.6 us)
Async XLA Ops:
  6.5 87.7 %copy-start = (bf16[16,1,384,128]{3,2,1,0:T(8,128)(2,1)S(1)}, bf16[16,1,384,128]{3,2,1,0:T(8,128)(2,1)}, u32[]{:S(2)}) copy-start(bf16[16,1,384,128]{3,2,1,0:T(8,128)(2,1)} %param.30) | copy-start | bytes 4718596
  6.5 20.6 %copy-start.1 = (bf16[16,2048]{1,0:T(8,128)(2,1)S(1)}, bf16[16,2048]{1,0:T(8,128)(2,1)}, u32[]{:S(2)}) copy-start(bf16[16,2048]{1,0:T(8,128)(2,1)} %param.23) | copy-start | bytes 196612
  6.5 20.7 %copy-start.13 = (s32[16]{0:T(128)S(1)}, s32[16]{0:T(128)}, u32[]{:S(2)}) copy-start(s32[16]{0:T(128)} %param.33) | copy-start | bytes 196
  6.5 20.8 %copy-start.4 = (f32[16,1,384]{2,1,0:T(1,128)S(1)}, f32[16,1,384]{2,1,0:T(1,128)}, u32[]{:S(2)}) copy-start(f32[16,1,384]{2,1,0:T(1,128)} %param.32) | copy-start | bytes 73732
  6.5 21.0 %copy-start.9 = (f32[2048]{0:T(1024)S(1)}, f32[2048]{0:T(1024)}, u32[]{:S(2)}) copy-start(f32[2048]{0:T(1024)} %param.24) | copy-start | bytes 24580
  6.5 21.1 %copy-start.16 = (bf16[2048,1]{0,1:T(2,128)(2,1)S(1)}, bf16[2048,1]{0,1:T(2,128)(2,1)}, u32[]{:S(2)}) copy-start(bf16[2048,1]{0,1:T(2,128)(2,1)} %param.28) | copy-start | bytes 12292
  6.6 84.8 %all-gather.4.cloned.1.call-start = ((), (), s32[]{:S(2)}) async-start(), calls=%async_computation.5 | async-start | bytes 1622016 | tf_op jit(solution)/shard_map/all_gather | solution.py:15
  9.7 86.3 %all-to-all-start = ((bf16[32,128,64]{1,2,0:T(8,128)(2,1)}), bf16[32,128,64]{1,2,0:T(8,128)(2,1)S(1)}, u32[]{:S(2)}, u32[]{:S(2)}) async-start(bf16[32,128,64]{1,2,0:T(8,128)(2,1)} %broadcast_in_dim.17), calls=%async_computation | async-start | bytes 1048576 | tf_op jit(solution)/shard_map/all_to_all | solution.py:21
  91.4 4.2 %copy-start.15 = (bf16[16,1,384,128]{3,2,1,0:T(8,128)(2,1)S(1)}, bf16[16,1,384,128]{3,2,1,0:T(8,128)(2,1)}, u32[]{:S(2)}) copy-start(bf16[16,1,384,128]{3,2,1,0:T(8,128)(2,1)} %param.31) | copy-start | bytes 4718596
  97.5 7.7 %copy-start.11 = (s32[16,2]{0,1:T(2,128)S(1)}, s32[16,2]{0,1:T(2,128)}, u32[]{:S(2)}) copy-start(s32[16,2]{0,1:T(2,128)} %param.40) | copy-start | bytes 388
  98.6 23.3 %copy-start.5 = (f32[2048]{0:T(1024)S(1)}, f32[2048]{0:T(1024)}, u32[]{:S(2)}) copy-start(f32[2048]{0:T(1024)} %param.35) | copy-start | bytes 24580
  98.6 23.0 %all-to-all-start.1 = ((bf16[16,16,2048]{2,1,0:T(8,128)(2,1)}), bf16[16,16,2048]{2,1,0:T(8,128)(2,1)S(1)}, u32[]{:S(2)}, u32[]{:S(2)}) async-start(bf16[16,16,2048]{2,1,0:T(8,128)(2,1)} %broadcast_in_dim.18), calls=%async_computation.1 | async-start | bytes 2097152 | tf_op jit(solution)/shard_map/all_to_all | solution.py:21
  105.2 28.1 %copy-start.7 = (bf16[64,128]{1,0:T(8,128)(2,1)S(1)}, bf16[64,128]{1,0:T(8,128)(2,1)}, u32[]{:S(2)}) copy-start(bf16[64,128]{1,0:T(8,128)(2,1)} %param.37) | copy-start | bytes 49156
  105.2 28.1 %copy-start.8 = (bf16[64,128]{1,0:T(8,128)(2,1)S(1)}, bf16[64,128]{1,0:T(8,128)(2,1)}, u32[]{:S(2)}) copy-start(bf16[64,128]{1,0:T(8,128)(2,1)} %param.36) | copy-start | bytes 49156
  105.3 28.7 %copy-start.10 = (bf16[2048]{0:T(1024)(128)(2,1)S(1)}, bf16[2048]{0:T(1024)(128)(2,1)}, u32[]{:S(2)}) copy-start(bf16[2048]{0:T(1024)(128)(2,1)} %param.39) | copy-start | bytes 12292
  105.3 28.8 %copy-start.6 = (bf16[128,64]{0,1:T(8,128)(2,1)S(1)}, bf16[128,64]{0,1:T(8,128)(2,1)}, u32[]{:S(2)}) copy-start(bf16[128,64]{0,1:T(8,128)(2,1)} %param.38) | copy-start | bytes 49156
  123.2 51.7 %copy-start.12 = (f32[16,2]{0,1:T(2,128)S(1)}, f32[16,2]{0,1:T(2,128)}, u32[]{:S(2)}) copy-start(f32[16,2]{0,1:T(2,128)} %param.42) | copy-start | bytes 388
  123.2 51.8 %all-to-all-start.2 = ((bf16[32,2,2048]{2,1,0:T(2,128)(2,1)}), bf16[32,2,2048]{2,1,0:T(2,128)(2,1)S(1)}, u32[]{:S(2)}, u32[]{:S(2)}) async-start(bf16[32,2,2048]{2,1,0:T(2,128)(2,1)} %reshape.216), calls=%async_computation.2 | async-start | bytes 524288 | tf_op jit(solution)/shard_map/all_to_all | solution.py:171
  133.2 72.6 %all-gather.6.cloned.1.call-start = ((), (), s32[]{:S(2)}) async-start(), calls=%async_computation.6 | async-start | bytes 1081344 | tf_op jit(solution)/shard_map/all_gather | solution.py:15
  134.0 41.0 %copy-start.2 = (bf16[1,2048,128]{2,1,0:T(8,128)(2,1)S(1)}, bf16[1,2048,128]{2,1,0:T(8,128)(2,1)}, u32[]{:S(2)}) copy-start(bf16[1,2048,128]{2,1,0:T(8,128)(2,1)} %param.43) | copy-start | bytes 1572868
  175.1 1.5 copy-start.3
  175.1 13.4 %copy-start.14 = (f32[16]{0:T(128)S(1)}, f32[16]{0:T(128)}, u32[]{:S(2)}) copy-start(f32[16]{0:T(128)} %param.41) | copy-start | bytes 196
  177.8 33.2 %all-to-all-start.3 = ((bf16[32,2,2048]{2,1,0:T(2,128)(2,1)}), bf16[32,2,2048]{2,1,0:T(2,128)(2,1)S(1)}, u32[]{:S(2)}, u32[]{:S(2)}) async-start(bf16[32,2,2048]{2,1,0:T(2,128)(2,1)} %copy.64), calls=%async_computation.3 | async-start | bytes 524288 | tf_op jit(solution)/shard_map/all_to_all | solution.py:178
Sparse Core Ops, SparseCore 0:
  9.5 81.8 all-gather.3
  136.2 69.6 all-gather.5
where the time goes:
time: 241 us; the launch traced here: 240 us
  waiting for transfers between devices  100 us (41%)
  blocking collectives  59.3 us (25%)
  starting transfers between devices  44.1 us (18%)
  between operations  14.4 us (6%)
  matrix products  10.6 us (4%)
  local copies, waits for them, and re-layouts  6.76 us (3%)
  other arithmetic  4.7 us (2%)
    all_gather x2, waiting for transfers between devices, sent_together(): filled = lax.all_gather(both, axis, axis=dim, tiled=True)  80.8 us
    all_gather x2, blocking collectives, gather_in_order(): pieces = lax.all_gather(pieces, axes[k], axis=0, tiled=True)  40.6 us
    all_to_all x2, starting transfers between devices, from_everyone(): return lax.all_to_all(copies, axis, split_axis=0, concat_axis=0, tiled=True)  23.3 us
    all_to_all x1, blocking collectives, from_everyone(): return lax.all_to_all(copies, axis, split_axis=0, concat_axis=0, tiled=True)  18.7 us
    all_to_all x2, waiting for transfers between devices, from_everyone(): return lax.all_to_all(copies, axis, split_axis=0, concat_axis=0, tiled=True)  15.7 us
    all_to_all x1, starting transfers between devices, shards(): lax.all_to_all(partial_out.reshape(sources, slots_now, feature).astype(jn...  10.6 us
    all_to_all x1, starting transfers between devices, shards(): lax.all_to_all(outbound, EP, split_axis=0, concat_axis=0, tiled=True)  10.1 us
  transfers between devices with their start and end apart: 6, of which 4 were waited for; matrix products, arithmetic and copies ran while one was open for 5% of the time, Pallas kernels for 0%

commit v1 on v0

--- a/solution.py
+++ b/solution.py
@@ -4,6 +4,7 @@
 from jax import lax
 from jax.sharding import Mesh
 from jax.sharding import PartitionSpec as P
+from jax.lax import all_to_all, axis_size
 
 EP = ("ep_0", "ep_1")
 EPSILON = 1e-06
@@ -40,7 +41,11 @@
 def gather_in_order(array, axes, sequence):
     pieces = array[None]
     for k in sequence:
-        pieces = lax.all_gather(pieces, axes[k], axis=0, tiled=True)
+        local = axes[k]
+        pieces = jnp.concatenate(
+            all_to_all(jnp.stack([pieces for _ in range(axis_size(local))], axis=0), local, 0, 0),
+            axis=0,
+        )
     held = [lax.axis_size(axes[k]) for k in reversed(sequence)]
     pieces = pieces.reshape(*held, *array.shape)
     turned = sorted(range(len(sequence)), key=lambda place: sequence[len(sequence) - 1 - place])

time: 241 us -> 265 us (1.100)
  waiting for transfers between devices: 100 us -> 153 us
  blocking collectives: 59.3 us -> 22.4 us
  starting transfers between devices: 44.1 us -> 50.6 us
    all_gather x2 -> x0, blocking collectives: 40.6 us -> none  [gather_in_order(): pieces = lax.all_gather(pieces, axes[k], axis=0, tiled=True)]
    all_gather x2, waiting for transfers between devices: 80.8 us -> 105 us  [sent_together(): filled = lax.all_gather(both, axis, axis=dim, tiled=True)]
    all_to_all x1, waiting for transfers between devices: 0.01 us -> 20.6 us  [shards(): lax.all_to_all(outbound, EP, split_axis=0, concat_axis=0, tiled=True)]
    all_to_all x0 -> x2, starting transfers between devices: none -> 11.3 us  [gather_in_order(): all_to_all(jnp.stack([pieces for _ in range(axis_size(local))], axis=0),...]
    all_to_all x0 -> x2, waiting for transfers between devices: none -> 11.2 us  [gather_in_order(): all_to_all(jnp.stack([pieces for _ in range(axis_size(local))], axis=0),...]
    all_to_all x1, starting transfers between devices: 10.6 us -> 3.65 us  [shards(): lax.all_to_all(partial_out.reshape(sources, slots_now, feature).astype(jn...]
    all_to_all x1, waiting for transfers between devices: 3.85 us -> 0.01 us  [shards(): lax.all_to_all(partial_out.reshape(sources, slots_now, feature).astype(jn...]
    all_to_all x1, blocking collectives: 18.7 us -> 22.4 us  [from_everyone(): return lax.all_to_all(copies, axis, split_axis=0, concat_axis=0, tiled=True)]
  transfers between devices with their start and end apart: 6 -> 8, of which waited for: 4 -> 5; matrix products, arithmetic and copies ran while one was open for 5% -> 6% of each run, Pallas kernels for 0% -> 0%
where the time goes in v1:
time: 265 us; the launch traced here: 264 us
  waiting for transfers between devices  153 us (58%)
  starting transfers between devices  50.6 us (19%)
  blocking collectives  22.4 us (8%)
  between operations  14.4 us (5%)
  matrix products  10.6 us (4%)
  local copies, waits for them, and re-layouts  7.3 us (3%)
  other arithmetic  5.54 us (2%)
    all_gather x2, waiting for transfers between devices, sent_together(): filled = lax.all_gather(both, axis, axis=dim, tiled=True)  105 us
    all_to_all x2, starting transfers between devices, from_everyone(): return lax.all_to_all(copies, axis, split_axis=0, concat_axis=0, tiled=True)  23.1 us
    all_to_all x1, blocking collectives, from_everyone(): return lax.all_to_all(copies, axis, split_axis=0, concat_axis=0, tiled=True)  22.4 us
    all_to_all x1, waiting for transfers between devices, shards(): lax.all_to_all(outbound, EP, split_axis=0, concat_axis=0, tiled=True)  20.6 us
    all_to_all x2, waiting for transfers between devices, from_everyone(): return lax.all_to_all(copies, axis, split_axis=0, concat_axis=0, tiled=True)  15.7 us
    all_to_all x1, starting transfers between devices, shards(): lax.all_to_all(outbound, EP, split_axis=0, concat_axis=0, tiled=True)  12.4 us
    all_to_all x2, starting transfers between devices, gather_in_order(): all_to_all(jnp.stack([pieces for _ in range(axis_size(local))], axis=0),...  11.3 us
    all_to_all x2, waiting for transfers between devices, gather_in_order(): all_to_all(jnp.stack([pieces for _ in range(axis_size(local))], axis=0),...  11.2 us
  transfers between devices with their start and end apart: 8, of which 5 were waited for; matrix products, arithmetic and copies ran while one was open for 6% of the time, Pallas kernels for 0%

profile of v1, /device:TPU:1, one launch (start us, length us, event | category | flops | bytes accessed | tf_op | source)
XLA Modules:
  0.0 263.8 jit_solution(5826213617477435574)
XLA Ops:
  6.6 1.5 pad_maximum_fusion.1
  8.1 1.6 broadcast_in_dim.15
  9.8 16.7 %all-to-all-start = ((bf16[32,128,64]{1,2,0:T(8,128)(2,1)}), bf16[32,128,64]{1,2,0:T(8,128)(2,1)S(1)}, u32[]{:S(2)}, u32[]{:S(2)}) async-start(bf16[32,128,64]{1,2,0:T(8,128)(2,1)} %broadcast_in_dim.15), calls=%async_computation | async-start | bytes 1048576 | tf_op jit(solution)/shard_map/all_to_all | solution.py:22
  27.2 0.1 fusion.33
  27.3 0.3 fusion.45
  27.6 0.2 fusion.65
  27.8 63.7 %all-gather.3.cloned.1.call-done = bf16[2048,384]{1,0:T(8,128)(2,1)} async-done(((bf16[64,384]{1,0:T(8,128)(2,1)}), bf16[2048,384]{1,0:T(8,128)(2,1)}) %all-gather.3.cloned.1.call-update) | async-done | bytes 1572880 | tf_op jit(solution)/shard_map/all_gather | solution.py:16
  91.5 1.4 convolution_convert_fusion.5
  92.9 1.4 fusion.14
  94.3 0.6 fusion.4
  95.0 0.3 fusion.82
  95.4 0.3 fusion.70
  95.7 0.4 fusion.2
  96.1 1.5 convolution_convert_fusion.2
  97.7 1.1 broadcast_in_dim.16
  98.8 6.4 %all-to-all-start.1 = ((bf16[16,16,2048]{2,1,0:T(8,128)(2,1)}), bf16[16,16,2048]{2,1,0:T(8,128)(2,1)S(1)}, u32[]{:S(2)}, u32[]{:S(2)}) async-start(bf16[16,16,2048]{2,1,0:T(8,128)(2,1)} %broadcast_in_dim.16), calls=%async_computation.1 | async-start | bytes 2097152 | tf_op jit(solution)/shard_map/all_to_all | solution.py:22
  105.3 0.1 eq.65
  105.5 0.2 select_reduce_fusion
  105.8 0.1 copy.48
  105.8 15.7 %all-to-all-done.1 = bf16[16,16,2048]{2,1,0:T(8,128)(2,1)S(1)} async-done(((bf16[16,16,2048]{2,1,0:T(8,128)(2,1)}), bf16[16,16,2048]{2,1,0:T(8,128)(2,1)S(1)}, u32[]{:S(2)}, u32[]{:S(2)}) %all-to-all-start.1) | async-done | bytes 1048608 | tf_op jit(solution)/shard_map/all_to_all | solution.py:22
  121.6 0.7 stack.6
  122.3 7.2 %all-to-all-start.4 = ((bf16[16,1,128,64]{2,3,1,0:T(8,128)(2,1)}), bf16[16,1,128,64]{2,3,1,0:T(8,128)(2,1)S(1)}, u32[]{:S(2)}, u32[]{:S(2)}) async-start(bf16[16,1,128,64]{2,3,1,0:T(8,128)(2,1)} %stack.6), calls=%async_computation.4 | async-start | bytes 524288 | tf_op jit(solution)/shard_map/all_to_all | solution.py:46
  129.6 0.1 convert_reduce_fusion.1
  129.7 0.1 fusion.37
  129.9 0.3 convolution_convert_fusion.1
  130.2 0.9 reshape.215
  131.1 11.2 %all-to-all-done.4 = bf16[16,1,128,64]{2,3,1,0:T(8,128)(2,1)S(1)} async-done(((bf16[16,1,128,64]{2,3,1,0:T(8,128)(2,1)}), bf16[16,1,128,64]{2,3,1,0:T(8,128)(2,1)S(1)}, u32[]{:S(2)}, u32[]{:S(2)}) %all-to-all-start.4) | async-done | bytes 262176 | tf_op jit(solution)/shard_map/all_to_all | solution.py:46
  142.3 12.4 %all-to-all-start.2 = ((bf16[32,2,2048]{2,1,0:T(2,128)(2,1)}), bf16[32,2,2048]{2,1,0:T(2,128)(2,1)S(1)}, u32[]{:S(2)}, u32[]{:S(2)}) async-start(bf16[32,2,2048]{2,1,0:T(2,128)(2,1)} %reshape.215), calls=%async_computation.2 | async-start | bytes 524288 | tf_op jit(solution)/shard_map/all_to_all | solution.py:176
  154.8 0.6 pad_maximum_fusion.2
  155.5 0.8 pad_maximum_fusion
  156.4 20.6 %all-to-all-done.2 = bf16[32,2,2048]{2,1,0:T(2,128)(2,1)S(1)} async-done(((bf16[32,2,2048]{2,1,0:T(2,128)(2,1)}), bf16[32,2,2048]{2,1,0:T(2,128)(2,1)S(1)}, u32[]{:S(2)}, u32[]{:S(2)}) %all-to-all-start.2) | async-done | bytes 262176 | tf_op jit(solution)/shard_map/all_to_all | solution.py:176
  177.0 4.1 %all-to-all-start.5 = ((bf16[2,16,128,64]{2,3,1,0:T(8,128)(2,1)}), bf16[2,16,128,64]{2,3,1,0:T(8,128)(2,1)S(1)}, u32[]{:S(2)}, u32[]{:S(2)}) async-start(bf16[2,16,128,64]{2,3,1,0:T(8,128)(2,1)} %pad_maximum_fusion), calls=%async_computation.5 | async-start | bytes 1048576 | tf_op jit(solution)/shard_map/all_to_all | solution.py:46
  181.1 0.1 reshape.216
  181.2 0.2 fusion.31
  181.5 1.3 fusion.6
  182.7 0.2 convolution_convert_fusion
  183.0 1.0 copy.50
  183.9 3.7 %all-to-all-start.3 = ((bf16[32,2,2048]{2,1,0:T(2,128)(2,1)}), bf16[32,2,2048]{2,1,0:T(2,128)(2,1)S(1)}, u32[]{:S(2)}, u32[]{:S(2)}) async-start(bf16[32,2,2048]{2,1,0:T(2,128)(2,1)} %copy.50), calls=%async_computation.3 | async-start | bytes 524288 | tf_op jit(solution)/shard_map/all_to_all | solution.py:183
  187.7 0.2 fusion.18
  187.9 41.7 %all-gather.5.cloned.1.call-done = bf16[2048,256]{1,0:T(8,128)(2,1)} async-done(((bf16[64,256]{1,0:T(8,128)(2,1)}), bf16[2048,256]{1,0:T(8,128)(2,1)}) %all-gather.5.cloned.1.call-update) | async-done | bytes 1048592 | tf_op jit(solution)/shard_map/all_gather | solution.py:16
  229.6 1.3 fusion.23
  231.0 0.6 gather_fusion
  231.6 0.6 gather_fusion.1
  232.2 1.5 fusion.1
  233.7 0.1 broadcast_in_dim.17
  233.8 22.4 %all_to_all.35 = bf16[16,16,2048]{2,1,0:T(8,128)(2,1)S(1)} all-to-all(bf16[16,16,2048]{2,1,0:T(8,128)(2,1)S(1)} %broadcast_in_dim.17), channel_id=1, replica_groups=mesh['ep_0'=16,'ep_1'=2,'tp'=16] {'tp'}, dimensions={0} | all-to-all | bytes 2097152 | tf_op jit(solution)/shard_map/all_to_all | solution.py:22
  256.2 0.1 convert_reduce_fusion
  256.3 0.6 fusion.40
  (60 shorter events, 0.8 us)
Async XLA Ops:
  6.5 87.8 %copy-start = (bf16[16,1,384,128]{3,2,1,0:T(8,128)(2,1)S(1)}, bf16[16,1,384,128]{3,2,1,0:T(8,128)(2,1)}, u32[]{:S(2)}) copy-start(bf16[16,1,384,128]{3,2,1,0:T(8,128)(2,1)} %param.30) | copy-start | bytes 4718596
  6.5 20.6 %copy-start.1 = (bf16[16,2048]{1,0:T(8,128)(2,1)S(1)}, bf16[16,2048]{1,0:T(8,128)(2,1)}, u32[]{:S(2)}) copy-start(bf16[16,2048]{1,0:T(8,128)(2,1)} %param.23) | copy-start | bytes 196612
  6.5 20.7 %copy-start.13 = (s32[16]{0:T(128)S(1)}, s32[16]{0:T(128)}, u32[]{:S(2)}) copy-start(s32[16]{0:T(128)} %param.33) | copy-start | bytes 196
  6.5 20.8 %copy-start.4 = (f32[16,1,384]{2,1,0:T(1,128)S(1)}, f32[16,1,384]{2,1,0:T(1,128)}, u32[]{:S(2)}) copy-start(f32[16,1,384]{2,1,0:T(1,128)} %param.32) | copy-start | bytes 73732
  6.5 21.1 %copy-start.9 = (f32[2048]{0:T(1024)S(1)}, f32[2048]{0:T(1024)}, u32[]{:S(2)}) copy-start(f32[2048]{0:T(1024)} %param.24) | copy-start | bytes 24580
  6.5 21.1 %copy-start.16 = (bf16[2048,1]{0,1:T(2,128)(2,1)S(1)}, bf16[2048,1]{0,1:T(2,128)(2,1)}, u32[]{:S(2)}) copy-start(bf16[2048,1]{0,1:T(2,128)(2,1)} %param.28) | copy-start | bytes 12292
  6.6 85.0 %all-gather.3.cloned.1.call-start = ((), (), s32[]{:S(2)}) async-start(), calls=%async_computation.7 | async-start | bytes 1622016 | tf_op jit(solution)/shard_map/all_gather | solution.py:16
  9.8 86.4 %all-to-all-start = ((bf16[32,128,64]{1,2,0:T(8,128)(2,1)}), bf16[32,128,64]{1,2,0:T(8,128)(2,1)S(1)}, u32[]{:S(2)}, u32[]{:S(2)}) async-start(bf16[32,128,64]{1,2,0:T(8,128)(2,1)} %broadcast_in_dim.15), calls=%async_computation | async-start | bytes 1048576 | tf_op jit(solution)/shard_map/all_to_all | solution.py:22
  91.5 4.2 %copy-start.15 = (bf16[16,1,384,128]{3,2,1,0:T(8,128)(2,1)S(1)}, bf16[16,1,384,128]{3,2,1,0:T(8,128)(2,1)}, u32[]{:S(2)}) copy-start(bf16[16,1,384,128]{3,2,1,0:T(8,128)(2,1)} %param.31) | copy-start | bytes 4718596
  97.6 7.5 %copy-start.11 = (s32[16,2]{0,1:T(2,128)S(1)}, s32[16,2]{0,1:T(2,128)}, u32[]{:S(2)}) copy-start(s32[16,2]{0,1:T(2,128)} %param.40) | copy-start | bytes 388
  97.6 23.9 %copy-start.6 = (bf16[128,64]{0,1:T(8,128)(2,1)S(1)}, bf16[128,64]{0,1:T(8,128)(2,1)}, u32[]{:S(2)}) copy-start(bf16[128,64]{0,1:T(8,128)(2,1)} %param.38) | copy-start | bytes 49156
  98.8 22.8 %all-to-all-start.1 = ((bf16[16,16,2048]{2,1,0:T(8,128)(2,1)}), bf16[16,16,2048]{2,1,0:T(8,128)(2,1)S(1)}, u32[]{:S(2)}, u32[]{:S(2)}) async-start(bf16[16,16,2048]{2,1,0:T(8,128)(2,1)} %broadcast_in_dim.16), calls=%async_computation.1 | async-start | bytes 2097152 | tf_op jit(solution)/shard_map/all_to_all | solution.py:22
  105.2 24.7 %copy-start.5 = (f32[2048]{0:T(1024)S(1)}, f32[2048]{0:T(1024)}, u32[]{:S(2)}) copy-start(f32[2048]{0:T(1024)} %param.35) | copy-start | bytes 24580
  122.3 32.4 %copy-start.7 = (bf16[64,128]{1,0:T(8,128)(2,1)S(1)}, bf16[64,128]{1,0:T(8,128)(2,1)}, u32[]{:S(2)}) copy-start(bf16[64,128]{1,0:T(8,128)(2,1)} %param.37) | copy-start | bytes 49156
  122.3 32.4 %copy-start.8 = (bf16[64,128]{1,0:T(8,128)(2,1)S(1)}, bf16[64,128]{1,0:T(8,128)(2,1)}, u32[]{:S(2)}) copy-start(bf16[64,128]{1,0:T(8,128)(2,1)} %param.36) | copy-start | bytes 49156
  122.3 19.9 %all-to-all-start.4 = ((bf16[16,1,128,64]{2,3,1,0:T(8,128)(2,1)}), bf16[16,1,128,64]{2,3,1,0:T(8,128)(2,1)S(1)}, u32[]{:S(2)}, u32[]{:S(2)}) async-start(bf16[16,1,128,64]{2,3,1,0:T(8,128)(2,1)} %stack.6), calls=%async_computation.4 | async-start | bytes 524288 | tf_op jit(solution)/shard_map/all_to_all | solution.py:46
  129.5 25.9 %copy-start.10 = (bf16[2048]{0:T(1024)(128)(2,1)S(1)}, bf16[2048]{0:T(1024)(128)(2,1)}, u32[]{:S(2)}) copy-start(bf16[2048]{0:T(1024)(128)(2,1)} %param.39) | copy-start | bytes 12292
  129.6 25.9 %copy-start.12 = (f32[16,2]{0,1:T(2,128)S(1)}, f32[16,2]{0,1:T(2,128)}, u32[]{:S(2)}) copy-start(f32[16,2]{0,1:T(2,128)} %param.42) | copy-start | bytes 388
  131.1 50.1 %copy-start.2 = (bf16[1,2048,128]{2,1,0:T(8,128)(2,1)S(1)}, bf16[1,2048,128]{2,1,0:T(8,128)(2,1)}, u32[]{:S(2)}) copy-start(bf16[1,2048,128]{2,1,0:T(8,128)(2,1)} %param.43) | copy-start | bytes 1572868
  142.3 34.7 %all-to-all-start.2 = ((bf16[32,2,2048]{2,1,0:T(2,128)(2,1)}), bf16[32,2,2048]{2,1,0:T(2,128)(2,1)S(1)}, u32[]{:S(2)}, u32[]{:S(2)}) async-start(bf16[32,2,2048]{2,1,0:T(2,128)(2,1)} %reshape.215), calls=%async_computation.2 | async-start | bytes 524288 | tf_op jit(solution)/shard_map/all_to_all | solution.py:176
  154.7 74.9 %all-gather.5.cloned.1.call-start = ((), (), s32[]{:S(2)}) async-start(), calls=%async_computation.8 | async-start | bytes 1081344 | tf_op jit(solution)/shard_map/all_gather | solution.py:16
  177.0 7.0 %all-to-all-start.5 = ((bf16[2,16,128,64]{2,3,1,0:T(8,128)(2,1)}), bf16[2,16,128,64]{2,3,1,0:T(8,128)(2,1)S(1)}, u32[]{:S(2)}, u32[]{:S(2)}) async-start(bf16[2,16,128,64]{2,3,1,0:T(8,128)(2,1)} %pad_maximum_fusion), calls=%async_computation.5 | async-start | bytes 1048576 | tf_op jit(solution)/shard_map/all_to_all | solution.py:46
  181.2 1.5 copy-start.3
  181.2 6.4 %copy-start.14 = (f32[16]{0:T(128)S(1)}, f32[16]{0:T(128)}, u32[]{:S(2)}) copy-start(f32[16]{0:T(128)} %param.41) | copy-start | bytes 196
  183.9 46.9 %all-to-all-start.3 = ((bf16[32,2,2048]{2,1,0:T(2,128)(2,1)}), bf16[32,2,2048]{2,1,0:T(2,128)(2,1)S(1)}, u32[]{:S(2)}, u32[]{:S(2)}) async-start(bf16[32,2,2048]{2,1,0:T(2,128)(2,1)} %copy.50), calls=%async_computation.3 | async-start | bytes 524288 | tf_op jit(solution)/shard_map/all_to_all | solution.py:183
Sparse Core Ops, SparseCore 0:
  9.5 81.9 all-gather.2
  157.6 71.9 all-gather.4
